TPU v7x, 32 devices: a whole 2x2x4 slice. The times are simulated.
32 devices in a mesh: dp: 4 (over y, x), kv: 4 (over z), tp: 2 (over core).
Axes of the slice: x: 2, y: 2, z: 4, core: 2. Of those that a mesh axis runs over, the one named last changes fastest.
Arguments:
- tokens: bfloat16 [4, 1536, 2048], P('dp', 'kv'), may hold values from -21 to 21
- seq_lengths: int32 [4], P('dp'), may hold values from 1 to 1536, 2304 in all
- block_picks: int32 [4, 24, 4, 16], P('dp', 'kv', 'tp'), may hold values from -1 to 17, as said below
- w_query: bfloat16 [2048, 1024], P('kv', 'tp'), may hold values from -0.125 to 0.125
- w_key: bfloat16 [2048, 256], P('kv', 'tp'), may hold values from -0.125 to 0.125
- w_value: bfloat16 [2048, 256], P('kv', 'tp'), may hold values from -0.125 to 0.125
- w_gate: bfloat16 [2048, 32], replicated, may hold values from -0.125 to 0.125
- w_ckey: bfloat16 [4096, 64], replicated, may hold values from -0.09375 to 0.09375
- w_cvalue: bfloat16 [4096, 64], replicated, may hold values from -0.09375 to 0.09375
- w_out: bfloat16 [1024, 2048], P('tp', 'kv'), may hold values from -0.1875 to 0.1875
Outputs:
- attention_out: bfloat16 [4, 1536, 2048], P('dp', ('kv', 'tp'))
Inputs may be any that keep to these rules, and one draw needn't show every extreme that they name: `block_picks`: A query block's entries name distinct blocks that all lie in earlier spans of 384 positions, or are -1; the largest such block is named in every draw. For one span and one group, the entries of all its query blocks together name blocks of any one other span at most 2 times; this is reached in every draw.
All inputs are finite; a program needn't handle non-finite values. No bound on the sum of `seq_lengths` on one device may be relied on, other than what follows from the above.
Results may differ from a plain program's by a relative error of at most 0.01.
The roundings to bfloat16 on the way count: a program that leaves them out, or rounds other values in their place, can miss the bound.
Values may be sent and summed in bfloat16 or wider, within the bound.
A program may use at most 64 MiB of HBM per device.

v0:
```python
import jax
import jax.numpy as jnp
from jax import lax
from jax.sharding import PartitionSpec as P

HEADS = 16
HEAD = 64
BLK = 64
PICKS = 16


masked_low = -1e30


def body(
    tokens, seq_lengths, block_picks, w_query, w_key, w_value, w_gate, w_ckey, w_cvalue, w_out
):
    token_rows = tokens[0]
    tok_count = token_rows.shape[0]
    shard_index = lax.axis_index("kv")
    head_index = lax.axis_index("tp")
    group_count = w_key.shape[1] // HEAD
    head_count = w_query.shape[1] // HEAD
    per_group = head_count // group_count
    block_count = tok_count // BLK
    inv_scale = HEAD ** (-0.5)
    zero_query = jnp.zeros((tok_count, w_query.shape[1]), jnp.float32)
    zero_key = jnp.zeros((tok_count, w_key.shape[1]), jnp.float32)
    runnings = (zero_query, zero_key, zero_key)
    weight_pieces = (
        lax.all_gather(w_query, "kv", axis=0, tiled=True),
        lax.all_gather(w_key, "kv", axis=0, tiled=True),
        lax.all_gather(w_value, "kv", axis=0, tiled=True),
    )
    collected = []
    for running, weight_piece in zip(runnings, weight_pieces):
        collected.append(jnp.dot(token_rows, weight_piece, preferred_element_type=jnp.float32))
    query_sum, key_sum, value_sum = tuple(collected)
    queries = query_sum.astype(jnp.bfloat16).reshape(block_count, BLK, group_count, per_group, HEAD)
    key_blocks = (
        key_sum.astype(jnp.bfloat16)
        .reshape(block_count, BLK, group_count, HEAD)
        .transpose(0, 2, 1, 3)
    )
    value_blocks = (
        value_sum.astype(jnp.bfloat16)
        .reshape(block_count, BLK, group_count, HEAD)
        .transpose(0, 2, 1, 3)
    )
    gate_all = jax.nn.sigmoid(jnp.dot(token_rows, w_gate, preferred_element_type=jnp.float32))
    gate_local = lax.dynamic_slice_in_dim(
        gate_all.reshape(tok_count, 2, HEADS), head_index * head_count, head_count, 2
    )
    gate_local = gate_local.reshape(block_count, BLK, 2, group_count, per_group)
    ckeys = jnp.dot(
        key_blocks.reshape(block_count * group_count, BLK * HEAD),
        w_ckey,
        preferred_element_type=jnp.float32,
    ).astype(jnp.bfloat16)
    cvalues = jnp.dot(
        value_blocks.reshape(block_count * group_count, BLK * HEAD),
        w_cvalue,
        preferred_element_type=jnp.float32,
    ).astype(jnp.bfloat16)
    cpairs = jnp.concatenate([ckeys, cvalues], axis=-1).reshape(block_count, group_count, 2 * HEAD)
    pair_blocks = jnp.concatenate([key_blocks, value_blocks], axis=-1)
    chosen = block_picks[0]
    usable = chosen >= 0
    group_ids = jnp.arange(group_count, dtype=jnp.int32)
    every_pair, every_cpair = (
        lax.all_gather(pair_blocks, "kv", axis=0, tiled=True),
        lax.all_gather(cpairs, "kv", axis=0, tiled=True),
    )
    flat_pairs = every_pair.reshape(-1, BLK, 2 * HEAD)
    lookup = jnp.where(usable, chosen, 0) * group_count + group_ids[None, :, None]
    fetched = flat_pairs[lookup]
    comp_keys = every_cpair[..., :HEAD]
    comp_values = every_cpair[..., HEAD:]
    block_ends = jnp.arange(every_cpair.shape[0], dtype=jnp.int32) * BLK + (BLK - 1)
    causal = jnp.arange(BLK)[None, :] <= jnp.arange(BLK)[:, None]

    def attend(block_inputs):
        qblock, gblock, own_pair, far_pair, far_usable, block_index = block_inputs
        query_spots = shard_index * tok_count + block_index * BLK + jnp.arange(BLK, dtype=jnp.int32)
        comp_score = (
            jnp.einsum("tgpd,cgd->gtpc", qblock, comp_keys, preferred_element_type=jnp.float32)
            * inv_scale
        )
        visible = (block_ends[None, :] <= query_spots[:, None])[None, :, None, :]
        comp_score = jnp.where(visible, comp_score, masked_low)
        comp_top = jnp.max(comp_score, axis=-1, keepdims=True)
        comp_weight = jnp.where(visible, jnp.exp(comp_score - comp_top), 0.0)
        comp_sum = jnp.maximum(jnp.sum(comp_weight, axis=-1, keepdims=True), 1.0)
        comp_prob = (comp_weight / comp_sum).astype(jnp.bfloat16)
        comp_out = jnp.einsum(
            "gtpc,cgd->tgpd", comp_prob, comp_values, preferred_element_type=jnp.float32
        )
        far_pairs = far_pair.reshape(group_count, PICKS * BLK, 2 * HEAD)
        own_score = (
            jnp.einsum(
                "tgpd,gsd->gtps", qblock, own_pair[..., :HEAD], preferred_element_type=jnp.float32
            )
            * inv_scale
        )
        own_mask = causal[None, :, None, :]
        own_score = jnp.where(own_mask, own_score, masked_low)
        far_score = (
            jnp.einsum(
                "tgpd,gkd->gtpk", qblock, far_pairs[..., :HEAD], preferred_element_type=jnp.float32
            )
            * inv_scale
        )
        far_mask = jnp.repeat(far_usable, BLK, axis=-1)[:, None, None, :]
        far_score = jnp.where(far_mask, far_score, masked_low)
        score_top = jnp.maximum(
            jnp.max(own_score, axis=-1, keepdims=True), jnp.max(far_score, axis=-1, keepdims=True)
        )
        own_weight = jnp.where(own_mask, jnp.exp(own_score - score_top), 0.0)
        far_weight = jnp.where(far_mask, jnp.exp(far_score - score_top), 0.0)
        normalizer = jnp.sum(own_weight, axis=-1, keepdims=True) + jnp.sum(
            far_weight, axis=-1, keepdims=True
        )
        own_prob = (own_weight / normalizer).astype(jnp.bfloat16)
        far_prob = (far_weight / normalizer).astype(jnp.bfloat16)
        chosen_out = jnp.einsum(
            "gtps,gsd->tgpd", own_prob, own_pair[..., HEAD:], preferred_element_type=jnp.float32
        ) + jnp.einsum(
            "gtpk,gkd->tgpd", far_prob, far_pairs[..., HEAD:], preferred_element_type=jnp.float32
        )
        mixed_out = gblock[:, 0, :, :, None] * comp_out + gblock[:, 1, :, :, None] * chosen_out
        return mixed_out.astype(jnp.bfloat16)

    attended = lax.map(
        attend,
        (
            queries,
            gate_local,
            pair_blocks,
            fetched,
            usable,
            jnp.arange(block_count, dtype=jnp.int32),
        ),
    )
    attended = attended.reshape(tok_count, head_count * HEAD)
    out_full = lax.all_gather(w_out, "kv", axis=1, tiled=True)
    half_rows = tok_count // lax.axis_size("tp")
    summed = lax.psum_scatter(
        jnp.dot(attended, out_full, preferred_element_type=jnp.float32).astype(jnp.bfloat16),
        "tp",
        scatter_dimension=0,
        tiled=True,
    ).astype(jnp.float32)
    out_positions = (
        shard_index * tok_count + head_index * half_rows + jnp.arange(half_rows, dtype=jnp.int32)
    )
    live_rows = out_positions < seq_lengths[0]
    return jnp.where(live_rows[:, None], summed, 0.0).astype(jnp.bfloat16)[None]


def solution(mesh):
    return jax.shard_map(
        body,
        mesh=mesh,
        in_specs=(
            P("dp", "kv", None),
            P("dp"),
            P("dp", "kv", "tp", None),
            P("kv", "tp"),
            P("kv", "tp"),
            P("kv", "tp"),
            P(),
            P(),
            P(),
            P("tp", "kv"),
        ),
        out_specs=P("dp", ("kv", "tp"), None),
        check_vma=False,
    )
```

profile of v0, /device:TPU:23, one launch (start us, length us, event | category | flops | bytes accessed | tf_op | source)
XLA Modules:
  0.0 188.2 jit_solution(17101830072245210733)
XLA Ops:
  6.5 0.7 all-gather.3.cloned.1.call-update
  7.3 0.7 all-gather.5.cloned.1.call-update
  8.1 13.6 %all_gather.19 = bf16[2048,128]{1,0:T(8,128)(2,1)S(1)} all-gather(bf16[512,128]{1,0:T(8,128)(2,1)} %param.16), channel_id=1, replica_groups=mesh['dp'=4,'kv'=4,'tp'=2] {'kv'}, dimensions={0}, use_global_device_ids=true | all-gather | bytes 655360 | tf_op jit(solution)/shard_map/all_gather | solution.py:32
  21.7 0.6 fusion.43
  22.4 20.8 %all_gather.20 = bf16[2048,128]{1,0:T(8,128)(2,1)S(1)} all-gather(bf16[512,128]{1,0:T(8,128)(2,1)S(1)} %copy-done.3), channel_id=1, replica_groups=mesh['dp'=4,'kv'=4,'tp'=2] {'kv'}, dimensions={0}, use_global_device_ids=true | all-gather | bytes 655360 | tf_op jit(solution)/shard_map/all_gather | solution.py:33
  44.6 0.6 fusion.58
  45.3 27.7 %all_gather.22 = bf16[24,2,64,128]{3,2,1,0:T(8,128)(2,1)S(1)} all-gather(bf16[6,2,64,128]{3,2,1,0:T(8,128)(2,1)S(1)} %pad_maximum_fusion), channel_id=1, replica_groups=mesh['dp'=4,'kv'=4,'tp'=2] {'kv'}, dimensions={0}, use_global_device_ids=true | all-gather | bytes 983040 | tf_op jit(solution)/shard_map/all_gather | solution.py:71
  73.3 1.3 convolution_convert_fusion.2
  74.7 9.1 %all_gather.21 = bf16[24,2,128]{2,1,0:T(2,128)(2,1)S(1)} all-gather(bf16[6,2,128]{2,1,0:T(2,128)(2,1)S(1)} %reshape.147), channel_id=1, replica_groups=mesh['dp'=4,'kv'=4,'tp'=2] {'kv'}, dimensions={0}, use_global_device_ids=true | all-gather | bytes 15360 | tf_op jit(solution)/shard_map/all_gather | solution.py:72
  83.9 2.7 %gather_fusion = bf16[192,64,128]{2,1,0:T(8,128)(2,1)} fusion(bf16[48,64,128]{2,1,0:T(8,128)(2,1)S(1)} %bitcast.174, s32[1024]{0:T(1024)S(1)} %pad_clamp_fusion), kind=kCustom, calls=%fused_computation | custom fusion | bytes 6292224 | tf_op jit(solution)/shard_map/gather | solution.py:76
  86.7 2.7 %fusion.40 = bf16[384,512]{1,0:T(8,128)(2,1)S(1)} fusion(bf16[2048,512]{1,0:T(8,128)(2,1)} %all-gather.3.cloned.1.call-done, bf16[1,384,2048]{2,1,0:T(8,128)(2,1)S(1)} %copy-done), kind=kOutput, calls=%fused_computation.69 | convolution fusion | flops 805502976 | bytes 4063232 | tf_op jit(solution)/shard_map/dot_general | solution.py:37
  89.8 65.4 %while.14 = (s32[]{:T(128)}, bf16[6,64,2,4,64]{4,3,2,1,0:T(4,128)(2,1)}, f32[6,64,2,2,4]{1,0,4,3,2:T(8,128)S(1)}, s32[6]{0:T(128)S(1)}, s32[]{:T(128)}, /*index=...) while((s32[]{:T(128)}, ...), condition=%wide.region_7.8_spmd.clone.clone, body=%wide.region_0.7_spmd.clone.clone.sunk | while | flops 153700000 | bytes 18673140 | solution.py:133
  90.0 1.1 constant_dynamic-slice_fusion.9
  92.0 1.0 copy-done.1
  93.0 0.6 fusion.102
  93.7 1.0 fusion.103
  94.7 0.6 dynamic_slice.69
  96.5 0.9 fusion.98
  97.4 2.5 %fusion.104 = bf16[1,64,2,4,64]{4,1,3,2,0:T(8,128)(2,1)S(1)} fusion(f32[64,2,4,64]{3,0,2,1:T(8,128)} %fusion.98, f32[2,64,64,4]{1,2,3,0:T(8,128)} %fusion.103, f32[2,64,4,1024]{3,1,2,0:T(8,128)} %copy-done.1, f32[2,64,4]{1,2,0:T(4,128)S(1)} %add.172, f32[2,64,4]{1,2,0:T(4,128)S(1)} %max.28, pred[2,1024]{1,0:T(4,128)(4,1)S(1)} %broadcast_in_dim.226, ...), kind=kOutput, calls=%fused_computation.19.clone.1 | convolution fusion | flops 70385664 | bytes 2957312 | tf_op jit(solution)/shard_map/while/body/eval_jaxpr/gtpk,gkd->tgpd/dot_general | solution.py:127
  100.0 0.8 copy_dynamic-update-slice_fusion.2
  101.0 1.1 constant_dynamic-slice_fusion.9
  102.9 1.0 copy-done.1
  103.9 0.6 fusion.102
  104.7 1.0 fusion.103
  105.6 0.6 dynamic_slice.69
  107.4 0.9 fusion.98
  108.3 2.5 %fusion.104 = bf16[1,64,2,4,64]{4,1,3,2,0:T(8,128)(2,1)S(1)} fusion(f32[64,2,4,64]{3,0,2,1:T(8,128)} %fusion.98, f32[2,64,64,4]{1,2,3,0:T(8,128)} %fusion.103, f32[2,64,4,1024]{3,1,2,0:T(8,128)} %copy-done.1, f32[2,64,4]{1,2,0:T(4,128)S(1)} %add.172, f32[2,64,4]{1,2,0:T(4,128)S(1)} %max.28, pred[2,1024]{1,0:T(4,128)(4,1)S(1)} %broadcast_in_dim.226, ...), kind=kOutput, calls=%fused_computation.19.clone.1 | convolution fusion | flops 70385664 | bytes 2957312 | tf_op jit(solution)/shard_map/while/body/eval_jaxpr/gtpk,gkd->tgpd/dot_general | solution.py:127
  110.9 0.8 copy_dynamic-update-slice_fusion.2
  111.9 1.1 constant_dynamic-slice_fusion.9
  113.8 1.0 copy-done.1
  114.8 0.6 fusion.102
  115.6 1.0 fusion.103
  116.5 0.6 dynamic_slice.69
  118.3 0.9 fusion.98
  119.2 2.5 %fusion.104 = bf16[1,64,2,4,64]{4,1,3,2,0:T(8,128)(2,1)S(1)} fusion(f32[64,2,4,64]{3,0,2,1:T(8,128)} %fusion.98, f32[2,64,64,4]{1,2,3,0:T(8,128)} %fusion.103, f32[2,64,4,1024]{3,1,2,0:T(8,128)} %copy-done.1, f32[2,64,4]{1,2,0:T(4,128)S(1)} %add.172, f32[2,64,4]{1,2,0:T(4,128)S(1)} %max.28, pred[2,1024]{1,0:T(4,128)(4,1)S(1)} %broadcast_in_dim.226, ...), kind=kOutput, calls=%fused_computation.19.clone.1 | convolution fusion | flops 70385664 | bytes 2957312 | tf_op jit(solution)/shard_map/while/body/eval_jaxpr/gtpk,gkd->tgpd/dot_general | solution.py:127
  121.8 0.8 copy_dynamic-update-slice_fusion.2
  122.8 1.1 constant_dynamic-slice_fusion.9
  124.7 1.0 copy-done.1
  125.7 0.6 fusion.102
  126.5 1.0 fusion.103
  127.4 0.6 dynamic_slice.69
  129.2 0.9 fusion.98
  130.1 2.5 %fusion.104 = bf16[1,64,2,4,64]{4,1,3,2,0:T(8,128)(2,1)S(1)} fusion(f32[64,2,4,64]{3,0,2,1:T(8,128)} %fusion.98, f32[2,64,64,4]{1,2,3,0:T(8,128)} %fusion.103, f32[2,64,4,1024]{3,1,2,0:T(8,128)} %copy-done.1, f32[2,64,4]{1,2,0:T(4,128)S(1)} %add.172, f32[2,64,4]{1,2,0:T(4,128)S(1)} %max.28, pred[2,1024]{1,0:T(4,128)(4,1)S(1)} %broadcast_in_dim.226, ...), kind=kOutput, calls=%fused_computation.19.clone.1 | convolution fusion | flops 70385664 | bytes 2957312 | tf_op jit(solution)/shard_map/while/body/eval_jaxpr/gtpk,gkd->tgpd/dot_general | solution.py:127
  132.6 0.8 copy_dynamic-update-slice_fusion.2
  133.6 1.1 constant_dynamic-slice_fusion.9
  135.6 1.0 copy-done.1
  136.6 0.6 fusion.102
  137.3 1.0 fusion.103
  138.3 0.6 dynamic_slice.69
  140.1 0.9 fusion.98
  141.0 2.5 %fusion.104 = bf16[1,64,2,4,64]{4,1,3,2,0:T(8,128)(2,1)S(1)} fusion(f32[64,2,4,64]{3,0,2,1:T(8,128)} %fusion.98, f32[2,64,64,4]{1,2,3,0:T(8,128)} %fusion.103, f32[2,64,4,1024]{3,1,2,0:T(8,128)} %copy-done.1, f32[2,64,4]{1,2,0:T(4,128)S(1)} %add.172, f32[2,64,4]{1,2,0:T(4,128)S(1)} %max.28, pred[2,1024]{1,0:T(4,128)(4,1)S(1)} %broadcast_in_dim.226, ...), kind=kOutput, calls=%fused_computation.19.clone.1 | convolution fusion | flops 70385664 | bytes 2957312 | tf_op jit(solution)/shard_map/while/body/eval_jaxpr/gtpk,gkd->tgpd/dot_general | solution.py:127
  143.5 0.8 copy_dynamic-update-slice_fusion.2
  144.5 1.1 constant_dynamic-slice_fusion.9
  146.4 1.0 copy-done.1
  147.5 0.6 fusion.102
  148.2 1.0 fusion.103
  149.2 0.6 dynamic_slice.69
  150.9 0.9 fusion.98
  151.9 2.5 %fusion.104 = bf16[1,64,2,4,64]{4,1,3,2,0:T(8,128)(2,1)S(1)} fusion(f32[64,2,4,64]{3,0,2,1:T(8,128)} %fusion.98, f32[2,64,64,4]{1,2,3,0:T(8,128)} %fusion.103, f32[2,64,4,1024]{3,1,2,0:T(8,128)} %copy-done.1, f32[2,64,4]{1,2,0:T(4,128)S(1)} %add.172, f32[2,64,4]{1,2,0:T(4,128)S(1)} %max.28, pred[2,1024]{1,0:T(4,128)(4,1)S(1)} %broadcast_in_dim.226, ...), kind=kOutput, calls=%fused_computation.19.clone.1 | convolution fusion | flops 70385664 | bytes 2957312 | tf_op jit(solution)/shard_map/while/body/eval_jaxpr/gtpk,gkd->tgpd/dot_general | solution.py:127
  154.4 0.8 copy_dynamic-update-slice_fusion.2
  155.2 2.0 %reshape.149 = bf16[384,512]{1,0:T(8,128)(2,1)S(1)} reshape(bf16[6,64,2,4,64]{4,3,2,1,0:T(4,128)(2,1)} %get-tuple-element.157) | data formatting | bytes 786432 | tf_op jit(solution)/shard_map/reshape | solution.py:144
  157.3 3.7 %convolution_convert_fusion = bf16[384,2048]{1,0:T(8,128)(2,1)} fusion(bf16[384,512]{1,0:T(8,128)(2,1)S(1)} %reshape.149, bf16[512,2048]{1,0:T(8,128)(2,1)} %all-gather.5.cloned.1.call-done), kind=kOutput, calls=%fused_computation.59 | convolution fusion | flops 806092800 | bytes 4063232 | tf_op jit(solution)/shard_map/dot_general | solution.py:148
  161.7 17.7 %reduce-scatter.2.cloned.1.call-done = bf16[192,2048]{1,0:T(8,128)(2,1)} async-done(((bf16[384,2048]{1,0:T(8,128)(2,1)}), bf16[192,2048]{1,0:T(8,128)(2,1)}) %reduce-scatter.2.cloned.1.call-update) | async-done | bytes 786448 | tf_op jit(solution)/shard_map/reduce_scatter | solution.py:147
  179.4 2.2 %fusion.61 = bf16[1,192,2048]{2,1,0:T(8,128)(2,1)} fusion(bf16[192,2048]{1,0:T(8,128)(2,1)} %reduce-scatter.2.cloned.1.call-done, pred[192]{0:T(512)(128)(4,1)S(1)} %add_compare_fusion), kind=kLoop, calls=%fused_computation.78 | loop fusion | flops 1179648 | bytes 1573056 | tf_op jit(solution)/shard_map/broadcast_in_dim | solution.py:157
  (159 shorter events, 11.5 us)
Async XLA Ops:
  6.5 15.1 %copy-start = (bf16[1,384,2048]{2,1,0:T(8,128)(2,1)S(1)}, bf16[1,384,2048]{2,1,0:T(8,128)(2,1)}, u32[]{:S(2)}) copy-start(bf16[1,384,2048]{2,1,0:T(8,128)(2,1)} %param.12) | copy-start | bytes 4718596
  6.5 15.8 %copy-start.3 = (bf16[512,128]{1,0:T(8,128)(2,1)S(1)}, bf16[512,128]{1,0:T(8,128)(2,1)}, u32[]{:S(2)}) copy-start(bf16[512,128]{1,0:T(8,128)(2,1)} %param.17) | copy-start | bytes 393220
  6.5 80.1 %all-gather.3.cloned.1.call-start = ((), (), s32[]{:S(2)}) async-start(), calls=%async_computation.1 | async-start | bytes 2621440 | tf_op jit(solution)/shard_map/all_gather | solution.py:31
  7.3 150.0 %all-gather.5.cloned.1.call-start = ((), (), s32[]{:S(2)}) async-start(), calls=%async_computation.2 | async-start | bytes 2621440 | tf_op jit(solution)/shard_map/all_gather | solution.py:145
  8.0 171.4 %reduce-scatter.2.cloned.1.call-start = ((), (), s32[]{:S(2)}) async-start(), calls=%async_computation.3 | async-start | bytes 2359296 | tf_op jit(solution)/shard_map/reduce_scatter | solution.py:147
  43.2 1.3 copy-start.5
  43.2 1.4 copy-start.4
  44.0 29.1 %copy-start.2 = (bf16[4096,64]{0,1:T(8,128)(2,1)S(1)}, bf16[4096,64]{0,1:T(8,128)(2,1)}, u32[]{:S(2)}) copy-start(bf16[4096,64]{0,1:T(8,128)(2,1)} %param.20) | copy-start | bytes 1572868
  91.6 1.4 copy-start.1
  102.6 1.4 copy-start.1
  113.5 1.4 copy-start.1
  124.4 1.4 copy-start.1
  135.2 1.4 copy-start.1
  146.1 1.4 copy-start.1
Sparse Core Ops, SparseCore 0:
  8.9 67.4 all-gather.2
  78.0 44.2 all-gather.4
  161.1 18.2 reduce-scatter.1
where the time goes:
time: 190 us; the launch traced here: 188 us
  blocking collectives  71.2 us (37%)
  matrix products  42.1 us (22%)
  local copies, waits for them, and re-layouts  28.9 us (15%)
  waiting for transfers between devices  19.2 us (10%)
  between operations  14 us (7%)
  other arithmetic  7.93 us (4%)
  loops' own time  4.77 us (3%)
    all_gather x1, blocking collectives, body(): lax.all_gather(pair_blocks, 'kv', axis=0, tiled=True)  27.7 us
    all_gather x1, blocking collectives, body(): lax.all_gather(w_value, 'kv', axis=0, tiled=True)  20.8 us
    reduce_scatter x1, waiting for transfers between devices, body(): lax.psum_scatter(jnp.dot(attended, out_full, preferred_element_type=jnp.f...  17.7 us
    dot_general x6, matrix products, attend(): jnp.einsum('gtpk,gkd->tgpd', far_prob, far_pairs[..., HEAD:], preferred_e...  15.1 us
    all_gather x1, blocking collectives, body(): lax.all_gather(w_key, 'kv', axis=0, tiled=True)  13.6 us
    dynamic_slice x24, local copies, waits for them, and re-layouts, body(): lax.map(attend, (queries, gate_local, pair_blocks, fetched, usable, jnp.a...  10.7 us
    all_gather x1, blocking collectives, body(): lax.all_gather(cpairs, 'kv', axis=0, tiled=True)  9.1 us
    while x12, local copies, waits for them, and re-layouts  6.3 us
  transfers between devices with their start and end apart: 3, of which 1 were waited for; matrix products, arithmetic and copies ran while one was open for 35% of the time, Pallas kernels for 0%

commit v1 on v0

v1 whole, which is shorter than its diff:
```python
import functools

import jax
import jax.numpy as jnp
from jax import lax
from jax.experimental import pallas as pl
from jax.experimental.pallas import tpu as pltpu
from jax.sharding import PartitionSpec as P

HEAD = 64
BLK = 64
CAP = 2
LANES = 128
PAD = 16
masked_low = -1e30
BF = jnp.bfloat16
F32 = jnp.float32


class Ring:
    def __init__(self, sizes, buf, rows, sems, share):
        self.n, self.buf, self.share = sizes["kv"], buf, share
        self.me = lax.axis_index("kv")
        self.dp = lax.axis_index("dp")
        n = self.n
        if share:
            self.piece = rows // 4
            self.parity = lax.rem(self.dp + self.dp // 2, 2)
            self.plans = []
            for way in (0, 1):
                plan = []
                for step in range(1, n // 2 + 1):
                    if 2 * step == n:
                        plan.append([way])
                    else:
                        plan.append([0, 1] if way == 0 else [1, 0])
                self.plans.append(plan)
        else:
            self.piece = rows
            self.parity = 0
            self.plans = [[[0] for _ in range(1, n)], []]
        self.zs, self.zr, self.fs, self.fr = sems
        self.started = []

    def rows_of(self, parity, i):
        if not self.share:
            return pl.ds(0, self.piece)
        return pl.ds(pl.multiple_of((2 * parity + i) * self.piece, self.piece), self.piece)

    def hop(self, way, step, i):
        n = self.n
        sign = 1 if way == 0 else -1
        owner = lax.rem(self.me - sign * (step - 1) + n, n)
        target = lax.rem(self.me + sign + n, n)
        at = self.buf.at[owner, self.rows_of(self.parity, i)]
        return pltpu.make_async_remote_copy(
            src_ref=at,
            dst_ref=at,
            send_sem=self.zs.at[way, step - 1, i],
            recv_sem=self.zr.at[way, step - 1, i],
            device_id={"kv": target},
            device_id_type=pl.DeviceIdType.MESH,
        )

    def arrival(self, way, step, i):
        n = self.n
        sign = 1 if way == 0 else -1
        owner = lax.rem(self.me - sign * step + n, n)
        at = self.buf.at[owner, self.rows_of(self.parity, i)]
        return pltpu.make_async_remote_copy(
            src_ref=at,
            dst_ref=at,
            send_sem=self.zs.at[way, step - 1, i],
            recv_sem=self.zr.at[way, step - 1, i],
            device_id={"kv": lax.rem(self.me + sign + n, n)},
            device_id_type=pl.DeviceIdType.MESH,
        )

    def pass_on(self, way, step, i, parity):
        n = self.n
        sign = 1 if way == 0 else -1
        owner = lax.rem(self.me - sign * step + n, n)
        at = self.buf.at[owner, self.rows_of(parity, i)]
        bit = 1 if i == 0 else 2
        low = lax.rem(self.dp, 2)
        high = self.dp // 2
        other = (high * 2 + 1 - low) if bit == 1 else ((1 - high) * 2 + low)
        return pltpu.make_async_remote_copy(
            src_ref=at,
            dst_ref=at,
            send_sem=self.fs.at[way, step - 1, i],
            recv_sem=self.fr.at[way, step - 1, i],
            device_id={"dp": other},
            device_id_type=pl.DeviceIdType.MESH,
        )

    def items(self):
        out = []
        deep = max(len(p) for p in self.plans)
        for step in range(1, deep + 1):
            for rank in range(2):
                for way in (0, 1):
                    plan = self.plans[way]
                    if step <= len(plan) and rank < len(plan[step - 1]):
                        out.append((way, step, plan[step - 1][rank]))
        return out

    def begin(self):
        for way, step, i in self.items():
            if step == 1:
                self.hop(way, 1, i).start()

    def relay(self):
        for way, step, i in self.items():
            self.arrival(way, step, i).wait_recv()
            plan = self.plans[way]
            if step < len(plan) and i in plan[step]:
                self.hop(way, step + 1, i).start()
            if self.share:
                self.pass_on(way, step, i, self.parity).start()

    def finish(self):
        if self.share:
            for way, step, i in self.items():
                self.pass_on(way, step, i, 1 - self.parity).wait_recv()

    def drain(self):
        for way, step, i in self.items():
            self.hop(way, step, i).wait_send()
            if self.share:
                self.pass_on(way, step, i, self.parity).wait_send()


def kernel(
    sizes,
    share,
    seq_ref,
    picks_ref,
    tokens_ref,
    wq_ref,
    wk_ref,
    wv_ref,
    wg_ref,
    wck_ref,
    wcv_ref,
    wo_ref,
    out_ref,
    tok,
    wall,
    wout,
    wgate,
    wck,
    wcv,
    queries,
    kv32,
    kv_all,
    flat,
    comp_all,
    gates,
    att,
    near,
    sendbuf,
    recvbuf,
    slots,
    local_sem,
    qs1,
    qr1,
    qs2,
    qr2,
    os1,
    or1,
    os2,
    or2,
    ks,
    kr,
    cs,
    cr,
    ts,
    tr,
):
    n = sizes["kv"]
    me = lax.axis_index("kv")
    tp = lax.axis_index("tp")
    dp = lax.axis_index("dp")
    count = tok.shape[0]
    blocks = count // BLK
    width = tok.shape[1]
    qcols = wq_ref.shape[1]
    heads = qcols // HEAD
    groups = wk_ref.shape[1] // HEAD
    per_group = heads // groups
    all_heads = wg_ref.shape[1] // 2
    picks = picks_ref.shape[3]
    depth = slots.shape[2]
    half = count // 2
    MESH = pl.DeviceIdType.MESH

    locals_ = [
        pltpu.make_async_copy(wq_ref, wall.at[me, :, pl.ds(0, qcols)], local_sem.at[0]),
        pltpu.make_async_copy(wk_ref, wall.at[me, :, pl.ds(qcols, LANES)], local_sem.at[1]),
        pltpu.make_async_copy(wv_ref, wall.at[me, :, pl.ds(qcols + LANES, LANES)], local_sem.at[2]),
        pltpu.make_async_copy(wo_ref, wout.at[me], local_sem.at[3]),
        pltpu.make_async_copy(tokens_ref.at[0], tok, local_sem.at[4]),
        pltpu.make_async_copy(wg_ref, wgate, local_sem.at[5]),
        pltpu.make_async_copy(wck_ref, wck, local_sem.at[6]),
        pltpu.make_async_copy(wcv_ref, wcv, local_sem.at[7]),
    ]
    for copy in locals_:
        copy.start()

    barrier = pltpu.get_barrier_semaphore()
    greeted = 0
    for d in range(1, n):
        pl.semaphore_signal(barrier, inc=1, device_id={"kv": lax.rem(me + d, n)}, device_id_type=MESH)
        greeted += 1
    pl.semaphore_signal(barrier, inc=1, device_id={"tp": 1 - tp}, device_id_type=MESH)
    greeted += 1
    if share:
        low, high = lax.rem(dp, 2), dp // 2
        for other in (high * 2 + 1 - low, (1 - high) * 2 + low):
            pl.semaphore_signal(barrier, inc=1, device_id={"dp": other}, device_id_type=MESH)
            greeted += 1
    pl.semaphore_wait(barrier, greeted)

    ring = Ring(sizes, wall, wall.shape[1], (qs1, qr1, qs2, qr2), share)
    oring = Ring(sizes, wout, wout.shape[1], (os1, or1, os2, or2), share)
    for copy in locals_[:3]:
        copy.wait()
    ring.begin()

    @pl.loop(0, blocks)
    def _(b):
        for g in range(groups):
            entries = [picks_ref[0, b, g, k] for k in range(picks)]
            last = jnp.int32(2**30)
            for s in range(depth):
                best = jnp.int32(-1)
                for entry in entries:
                    best = jnp.maximum(best, jnp.where(entry < last, entry, -1))
                slots[b, g, s] = best
                last = best

    for copy in locals_[3:]:
        copy.wait()
    gates[...] = jax.nn.sigmoid(jnp.dot(tok[...], wgate[...], preferred_element_type=F32))
    ring.relay()
    oring.begin()
    ring.finish()

    every = wall[...].reshape(width, wall.shape[2])
    kvsum = jnp.dot(tok[...], every[:, qcols:], preferred_element_type=F32).astype(BF)
    kv_all[pl.ds(me * blocks, blocks)] = kvsum.reshape(blocks, BLK, 2 * LANES)
    kv32[0] = kvsum[:, :LANES].astype(F32)
    kv32[1] = kvsum[:, LANES:].astype(F32)
    qsum = jnp.dot(tok[...], every[:, :qcols], preferred_element_type=F32)
    queries[...] = qsum.astype(BF).astype(F32)

    def kv_copy(d, slot):
        return pltpu.make_async_remote_copy(
            src_ref=kv_all.at[pl.ds(slot * blocks, blocks)],
            dst_ref=kv_all.at[pl.ds(slot * blocks, blocks)],
            send_sem=ks.at[d],
            recv_sem=kr.at[d],
            device_id={"kv": lax.rem(me + d, n)},
            device_id_type=MESH,
        )

    def comp_copy(d, slot):
        return pltpu.make_async_remote_copy(
            src_ref=comp_all.at[slot],
            dst_ref=comp_all.at[slot],
            send_sem=cs.at[d],
            recv_sem=cr.at[d],
            device_id={"kv": lax.rem(me + d, n)},
            device_id_type=MESH,
        )

    for d in range(1, n):

        @pl.when(me + d < n)
        def _():
            kv_copy(d, me).start()

    left = lax.broadcasted_iota(jnp.int32, (blocks, LANES), 1) < HEAD
    parts = []
    for which, weights in ((0, wck), (1, wcv)):
        source = kv32.at[which]
        flat[...] = jnp.zeros_like(flat)
        for pair in range(BLK // 2):
            even = source[pl.ds(2 * pair, blocks, stride=BLK), :]
            odd = source[pl.ds(2 * pair + 1, blocks, stride=BLK), :]
            span = pl.ds(pair * LANES, LANES)
            flat[0, 0:blocks, span] = jnp.where(left, even, pltpu.roll(odd, HEAD, 1))
            flat[1, 0:blocks, span] = jnp.where(left, pltpu.roll(even, HEAD, 1), odd)
        for g in range(groups):
            parts.append(jnp.dot(flat[g].astype(BF), weights[...], preferred_element_type=F32))
    comp_all[me] = jnp.concatenate(parts, axis=1).astype(BF)
    for d in range(1, n):
        comp_copy(d, me).start()

    oring.relay()

    for d in range(1, n):

        @pl.when(me - d >= 0)
        def _():
            kv_copy(d, lax.rem(me - d + n, n)).wait_recv()

        comp_copy(d, lax.rem(me - d + n, n)).wait_recv()

    rows = per_group * BLK
    comp_pairs = comp_all[...].reshape(n * PAD, 2 * LANES)
    nkeys = (1 + depth) * BLK
    lane64 = lax.broadcasted_iota(jnp.int32, (BLK, LANES), 1) < HEAD
    dims = (((1,), (1,)), ((), ()))
    comp_lane = lax.broadcasted_iota(jnp.int32, (rows, n * PAD), 1)
    comp_spot = lax.rem(lax.broadcasted_iota(jnp.int32, (rows, n * PAD), 0), BLK)
    comp_block = (comp_lane // PAD) * blocks + lax.rem(comp_lane, PAD)
    comp_real = lax.rem(comp_lane, PAD) < blocks
    key_lane = lax.broadcasted_iota(jnp.int32, (1, nkeys), 1)
    own_lane = lax.broadcasted_iota(jnp.int32, (rows, nkeys), 1)
    own_spot = lax.rem(lax.broadcasted_iota(jnp.int32, (rows, nkeys), 0), BLK)
    hidden = jnp.logical_and(own_lane < BLK, own_lane > own_spot)

    for b in range(blocks):
        spot = pl.ds(b * BLK, BLK)
        for g in range(groups):
            stacked = []
            for i in range(per_group):
                h = g * per_group + i
                tile = queries[spot, pl.ds((h // 2) * LANES, LANES)] * (HEAD**-0.5)
                if h % 2 != g:
                    tile = pltpu.roll(tile, HEAD, 1)
                keep = lane64 if g == 0 else jnp.logical_not(lane64)
                stacked.append(jnp.where(keep, tile, 0.0))
            qrows = jnp.concatenate(stacked, axis=0).astype(BF)

            comp_score = lax.dot_general(qrows, comp_pairs[:, :LANES], dims, preferred_element_type=F32)
            visible = jnp.logical_and(
                comp_real, (comp_block + 1) * BLK - 1 <= me * count + b * BLK + comp_spot
            )
            comp_score = jnp.where(visible, comp_score, masked_low)
            comp_top = jnp.max(comp_score, axis=1, keepdims=True)
            comp_weight = jnp.where(visible, jnp.exp(comp_score - comp_top), 0.0)
            comp_sum = jnp.maximum(jnp.sum(comp_weight, axis=1, keepdims=True), 1.0)
            comp_prob = (comp_weight / comp_sum).astype(BF)
            comp_out = jnp.dot(comp_prob, comp_pairs[:, LANES:], preferred_element_type=F32)

            near[0:BLK, :] = kv_all[me * blocks + b]
            bias = jnp.zeros((1, nkeys), F32)
            named = [slots[b, g, s] for s in range(depth)]

            def pickup(c, held):
                block = kv_all[c]
                return tuple(lax.select(pick == c, block, old) for pick, old in zip(named, held))

            nothing = jnp.zeros((BLK, 2 * LANES), BF)
            found = lax.fori_loop(0, me * blocks, pickup, (nothing,) * depth)
            for s in range(depth):
                near[(s + 1) * BLK : (s + 2) * BLK, :] = found[s]
                shut = jnp.where(named[s] < 0, masked_low, 0.0)
                bias = jnp.where(key_lane // BLK == s + 1, shut, bias)
            score = lax.dot_general(qrows, near[:, :LANES], dims, preferred_element_type=F32) + bias
            score = jnp.where(hidden, masked_low, score)
            top = jnp.max(score, axis=1, keepdims=True)
            weight = jnp.exp(score - top)
            prob = (weight / jnp.sum(weight, axis=1, keepdims=True)).astype(BF)
            chosen_out = jnp.dot(prob, near[:, LANES:], preferred_element_type=F32)

            cols = [[], []]
            for i in range(per_group):
                for branch in (0, 1):
                    first = branch * all_heads + g * per_group + i
                    a = gates[spot, first : first + 1]
                    c = gates[spot, first + heads : first + heads + 1]
                    cols[branch].append(jnp.where(tp == 0, a, c))
            mixed = (
                jnp.concatenate(cols[0], axis=0) * comp_out
                + jnp.concatenate(cols[1], axis=0) * chosen_out
            )
            for j in range(per_group // 2):
                even = mixed[2 * j * BLK : (2 * j + 1) * BLK]
                odd = mixed[(2 * j + 1) * BLK : (2 * j + 2) * BLK]
                if g == 0:
                    odd = pltpu.roll(odd, HEAD, 1)
                else:
                    even = pltpu.roll(even, HEAD, 1)
                tile = g * (per_group // 2) + j
                att[spot, tile * LANES : (tile + 1) * LANES] = jnp.where(lane64, even, odd).astype(BF)

    oring.finish()

    def back(o):
        return pltpu.make_async_remote_copy(
            src_ref=sendbuf.at[o],
            dst_ref=recvbuf.at[o],
            send_sem=ts.at[o],
            recv_sem=tr.at[o],
            device_id={"tp": 1 - tp},
            device_id_type=MESH,
        )

    theirs = att[pl.ds(pl.multiple_of((1 - tp) * half, half), half), :]
    mine = att[pl.ds(pl.multiple_of(tp * half, half), half), :]
    for o in range(n):
        sendbuf[o] = jnp.dot(theirs, wout[o], preferred_element_type=F32).astype(BF)
        back(o).start()
    cols_each = wout.shape[2]
    live = (
        me * count + tp * half + lax.broadcasted_iota(jnp.int32, (half, cols_each), 0)
    ) < seq_ref[0]
    for o in range(n):
        kept = jnp.dot(mine, wout[o], preferred_element_type=F32).astype(BF).astype(F32)
        back(o).wait_recv()
        total = kept + recvbuf[o].astype(F32)
        out_ref[0, :, o * cols_each : (o + 1) * cols_each] = jnp.where(live, total, 0.0).astype(BF)

    ring.drain()
    oring.drain()
    for d in range(1, n):

        @pl.when(me + d < n)
        def _():
            kv_copy(d, me).wait_send()

        comp_copy(d, me).wait_send()
    for o in range(n):
        back(o).wait_send()


def solution(mesh):
    sizes = dict(mesh.shape)
    n = sizes["kv"]

    def body(tokens, seq_lengths, block_picks, wq, wk, wv, wg, wck, wcv, wo):
        _, count, width = tokens.shape
        blocks = count // BLK
        groups = wk.shape[1] // HEAD
        share = sizes["dp"] == 4 and (wq.shape[0] // 4) % 16 == 0 and n % 2 == 0
        steps = (2, n // 2, 2) if share else (1, n - 1, 1)
        depth = min(block_picks.shape[3], CAP * (n - 1))
        cols = wq.shape[1] + wk.shape[1] + wv.shape[1]
        half = count // sizes["tp"]
        sem = pltpu.SemaphoreType.DMA
        return pl.pallas_call(
            functools.partial(kernel, sizes, share),
            out_shape=jax.ShapeDtypeStruct((1, half, wo.shape[1] * n), BF),
            in_specs=[pl.BlockSpec(memory_space=pltpu.SMEM)] * 2
            + [pl.BlockSpec(memory_space=pl.ANY)] * 8,
            out_specs=pl.BlockSpec(memory_space=pltpu.VMEM),
            scratch_shapes=[
                pltpu.VMEM((count, width), BF),
                pltpu.VMEM((n, wq.shape[0], cols), BF),
                pltpu.VMEM((n,) + wo.shape, BF),
                pltpu.VMEM(wg.shape, BF),
                pltpu.VMEM(wck.shape, BF),
                pltpu.VMEM(wcv.shape, BF),
                pltpu.VMEM((count, wq.shape[1]), F32),
                pltpu.VMEM((2, count, LANES), F32),
                pltpu.VMEM((n * blocks, BLK, 2 * LANES), BF),
                pltpu.VMEM((groups, PAD, BLK * HEAD), F32),
                pltpu.VMEM((n, PAD, 2 * LANES), BF),
                pltpu.VMEM((count, wg.shape[1]), F32),
                pltpu.VMEM((count, wq.shape[1]), BF),
                pltpu.VMEM(((1 + depth) * BLK, 2 * LANES), BF),
                pltpu.VMEM((n, half, wo.shape[1]), BF),
                pltpu.VMEM((n, half, wo.shape[1]), BF),
                pltpu.SMEM((blocks, groups, depth), jnp.int32),
                sem((8,)),
            ]
            + [sem(steps)] * 8
            + [sem((n,))] * 6,
            compiler_params=pltpu.CompilerParams(
                collective_id=0, has_side_effects=True, vmem_limit_bytes=60 * 1024 * 1024
            ),
        )(seq_lengths, block_picks, tokens, wq, wk, wv, wg, wck, wcv, wo)

    return jax.shard_map(
        body,
        mesh=mesh,
        in_specs=(
            P("dp", "kv", None),
            P("dp"),
            P("dp", "kv", "tp", None),
            P("kv", "tp"),
            P("kv", "tp"),
            P("kv", "tp"),
            P(),
            P(),
            P(),
            P("tp", "kv"),
        ),
        out_specs=P("dp", ("kv", "tp"), None),
        check_vma=False,
    )
```

time: 190 us -> 93.8 us (0.49)
  Pallas kernels: 0 us -> 85 us
  blocking collectives: 71.2 us -> 0 us
  matrix products: 42.1 us -> 0 us
  local copies, waits for them, and re-layouts: 28.9 us -> 7.75 us
  waiting for transfers between devices: 19.2 us -> 0 us
  between operations: 14 us -> 0.72 us
  other arithmetic: 7.93 us -> 0 us
  loops' own time: 4.77 us -> 0 us
    pallas_call x0 -> x1, Pallas kernels: none -> 85 us  [body(): pl.pallas_call(functools.partial(kernel, sizes, share), out_shape=jax.Sha...]
    all_gather x4 -> x0, blocking collectives: 71.2 us -> none  [the longest x1 27.7 us: body(): lax.all_gather(pair_blocks, 'kv', axis=0, tiled=True)]
    dot_general x43 -> x0, matrix products: 42.1 us -> none  [the longest x6 15.1 us: attend(): jnp.einsum('gtpk,gkd->tgpd', far_prob, far_pairs[..., HEAD:], preferred_e...]
    reduce_scatter x1 -> x0, waiting for transfers between devices: 17.7 us -> none  [body(): lax.psum_scatter(jnp.dot(attended, out_full, preferred_element_type=jnp.f...]
    dynamic_slice x25 -> x0, local copies, waits for them, and re-layouts: 10.7 us -> none  [the longest x24 10.7 us: body(): lax.map(attend, (queries, gate_local, pair_blocks, fetched, usable, jnp.a...]
    unnamed x12 -> x6, local copies, waits for them, and re-layouts: 0.03 us -> 7.75 us
    while x12 -> x0, local copies, waits for them, and re-layouts: 6.3 us -> none
    another operation x1 -> x0, loops' own time: 4.77 us -> none  [body(): lax.map(attend, (queries, gate_local, pair_blocks, fetched, usable, jnp.a...]
  transfers between devices with their start and end apart: 3 -> 0, of which waited for: 1 -> 0; matrix products, arithmetic and copies ran while one was open for 35% -> 0% of each run, Pallas kernels for 0% -> 0%
where the time goes in v1:
time: 93.8 us; the launch traced here: 93.5 us
  Pallas kernels  85 us (91%)
  local copies, waits for them, and re-layouts  7.75 us (8%)
    pallas_call x1, Pallas kernels, body(): pl.pallas_call(functools.partial(kernel, sizes, share), out_shape=jax.Sha...  85 us
    unnamed x6, local copies, waits for them, and re-layouts  7.75 us

profile of v1, /device:TPU:23, one launch (start us, length us, event | category | flops | bytes accessed | tf_op | source)
XLA Modules:
  0.0 93.5 jit_solution(4584502083544006913)
XLA Ops:
  0.0 0.0 copy-start
  0.7 1.9 %copy.11.wg_ref = bf16[2048,32]{1,0:T(8,128)(2,1)} copy(bf16[2048,32]{0,1:T(8,128)(2,1)} %param.16) | data formatting | bytes 262144 | tf_op args[6]
  2.6 2.4 %copy.12.wck_ref = bf16[4096,64]{1,0:T(8,128)(2,1)} copy(bf16[4096,64]{0,1:T(8,128)(2,1)} %param.17) | data formatting | bytes 1048576 | tf_op args[7]
  5.0 0.0 copy-done
  5.0 1.4 %copy.13.wcv_ref = bf16[4096,64]{1,0:T(8,128)(2,1)} copy(bf16[4096,64]{0,1:T(8,128)(2,1)S(1)} %copy-done) | data formatting | bytes 1048576 | tf_op args[8]
  6.4 85.0 %shard_map.100 = bf16[1,192,2048]{2,1,0:T(8,128)(2,1)} custom-call(s32[1]{0:T(128)S(6)} %copy.15.seq_ref, s32[1,6,2,16]{3,2,1,0:T(2,128)} %picks_ref.1, bf16[1,384,2048]{2,1,0:T(8,128)(2,1)} %tokens_ref.1, bf16[512,512]{1,0:T(8,128)(2,1)} %wq_ref.1, bf16[512,128]{1,0:T(8,128)(2,1)} %wk_ref.1, bf16[512,128]{1,0:T(8,128)(2,1)} %wv_ref.1, ...), custom_call_target="tpu_custom_call" | custom-call | tf_op jit(solution)/shard_map/pallas_call | solution.py:445
  91.4 2.1 %copy.16 = bf16[1,192,2048]{2,1,0:T(8,128)(2,1)} copy(bf16[1,192,2048]{2,1,0:T(8,128)(2,1)} %shard_map.100) | data formatting | bytes 1572864
Async XLA Ops:
  0.0 5.0 %copy-start = (bf16[4096,64]{0,1:T(8,128)(2,1)S(1)}, bf16[4096,64]{0,1:T(8,128)(2,1)}, u32[]{:S(2)}) copy-start(bf16[4096,64]{0,1:T(8,128)(2,1)} %param.18) | copy-start | bytes 1572868

commit v2 on v1

--- a/solution.py
+++ b/solution.py
@@ -110,8 +110,8 @@
             if step == 1:
                 self.hop(way, 1, i).start()
 
-    def relay(self):
-        for way, step, i in self.items():
+    def relay(self, first=0, last=None):
+        for way, step, i in self.items()[first:last]:
             self.arrival(way, step, i).wait_recv()
             plan = self.plans[way]
             if step < len(plan) and i in plan[step]:
@@ -162,6 +162,7 @@
     sendbuf,
     recvbuf,
     slots,
+    shuts,
     local_sem,
     qs1,
     qr1,
@@ -189,11 +190,12 @@
     heads = qcols // HEAD
     groups = wk_ref.shape[1] // HEAD
     per_group = heads // groups
-    all_heads = wg_ref.shape[1] // 2
+    all_heads = wg_ref.shape[0] // 2
     picks = picks_ref.shape[3]
     depth = slots.shape[2]
     half = count // 2
     MESH = pl.DeviceIdType.MESH
+    dims = (((1,), (1,)), ((), ()))
 
     locals_ = [
         pltpu.make_async_copy(wq_ref, wall.at[me, :, pl.ds(0, qcols)], local_sem.at[0]),
@@ -228,21 +230,46 @@
         copy.wait()
     ring.begin()
 
+    together = CAP * (n - 1) <= picks
+    for g in range(groups if together else 0):
+        last = jnp.int32(2**30)
+        for s in range(depth):
+
+            def scan(b, best):
+                for k in range(picks):
+                    entry = picks_ref[0, b, g, k]
+                    best = jnp.maximum(best, jnp.where(entry < last, entry, -1))
+                return best
+
+            last = lax.fori_loop(0, blocks, scan, jnp.int32(-1))
+            slots[0, g, s] = last
+
     @pl.loop(0, blocks)
     def _(b):
         for g in range(groups):
             entries = [picks_ref[0, b, g, k] for k in range(picks)]
             last = jnp.int32(2**30)
             for s in range(depth):
-                best = jnp.int32(-1)
-                for entry in entries:
-                    best = jnp.maximum(best, jnp.where(entry < last, entry, -1))
-                slots[b, g, s] = best
-                last = best
+                if together:
+                    best = slots[0, g, s]
+                    hits = jnp.int32(0)
+                    for entry in entries:
+                        hits = jnp.maximum(hits, jnp.where(entry == best, 1, 0))
+                    hits = jnp.where(best < 0, 0, hits)
+                    shuts[b, g, s] = jnp.where(hits > 0, 0.0, masked_low)
+                else:
+                    best = jnp.int32(-1)
+                    for entry in entries:
+                        best = jnp.maximum(best, jnp.where(entry < last, entry, -1))
+                    slots[b, g, s] = best
+                    shuts[b, g, s] = jnp.where(best < 0, masked_low, 0.0)
+                    last = best
 
     for copy in locals_[3:]:
         copy.wait()
-    gates[...] = jax.nn.sigmoid(jnp.dot(tok[...], wgate[...], preferred_element_type=F32))
+    gates[...] = jax.nn.sigmoid(
+        lax.dot_general(tok[...], wgate[...], dims, preferred_element_type=F32)
+    )
     ring.relay()
     oring.begin()
     ring.finish()
@@ -293,12 +320,16 @@
             flat[0, 0:blocks, span] = jnp.where(left, even, pltpu.roll(odd, HEAD, 1))
             flat[1, 0:blocks, span] = jnp.where(left, pltpu.roll(even, HEAD, 1), odd)
         for g in range(groups):
-            parts.append(jnp.dot(flat[g].astype(BF), weights[...], preferred_element_type=F32))
+            parts.append(
+                lax.dot_general(flat[g].astype(BF), weights[...], dims, preferred_element_type=F32)
+            )
     comp_all[me] = jnp.concatenate(parts, axis=1).astype(BF)
     for d in range(1, n):
         comp_copy(d, me).start()
 
-    oring.relay()
+    late = len(oring.items())
+    early = 2 if share else late
+    oring.relay(0, early)
 
     for d in range(1, n):
 
@@ -312,7 +343,6 @@
     comp_pairs = comp_all[...].reshape(n * PAD, 2 * LANES)
     nkeys = (1 + depth) * BLK
     lane64 = lax.broadcasted_iota(jnp.int32, (BLK, LANES), 1) < HEAD
-    dims = (((1,), (1,)), ((), ()))
     comp_lane = lax.broadcasted_iota(jnp.int32, (rows, n * PAD), 1)
     comp_spot = lax.rem(lax.broadcasted_iota(jnp.int32, (rows, n * PAD), 0), BLK)
     comp_block = (comp_lane // PAD) * blocks + lax.rem(comp_lane, PAD)
@@ -322,8 +352,26 @@
     own_spot = lax.rem(lax.broadcasted_iota(jnp.int32, (rows, nkeys), 0), BLK)
     hidden = jnp.logical_and(own_lane < BLK, own_lane > own_spot)
 
+    def pick_up(b, g):
+        named = [slots[b, g, s] for s in range(depth)]
+
+        def scan(c, held):
+            block = kv_all[c]
+            return tuple(lax.select(pick == c, block, old) for pick, old in zip(named, held))
+
+        nothing = jnp.zeros((BLK, 2 * LANES), BF)
+        found = lax.fori_loop(0, me * blocks, scan, (nothing,) * depth)
+        for s in range(depth):
+            near[g, (s + 1) * BLK : (s + 2) * BLK, :] = found[s]
+
+    for g in range(groups if together else 0):
+        pick_up(0, g)
+
     for b in range(blocks):
         spot = pl.ds(b * BLK, BLK)
+        if b > 0 and early < late:
+            oring.relay(early, early + 1)
+            early += 1
         for g in range(groups):
             stacked = []
             for i in range(per_group):
@@ -343,29 +391,21 @@
             comp_top = jnp.max(comp_score, axis=1, keepdims=True)
             comp_weight = jnp.where(visible, jnp.exp(comp_score - comp_top), 0.0)
             comp_sum = jnp.maximum(jnp.sum(comp_weight, axis=1, keepdims=True), 1.0)
-            comp_prob = (comp_weight / comp_sum).astype(BF)
+            comp_prob = (comp_weight * (1.0 / comp_sum)).astype(BF)
             comp_out = jnp.dot(comp_prob, comp_pairs[:, LANES:], preferred_element_type=F32)
 
-            near[0:BLK, :] = kv_all[me * blocks + b]
+            if not together:
+                pick_up(b, g)
+            near[g, 0:BLK, :] = kv_all[me * blocks + b]
             bias = jnp.zeros((1, nkeys), F32)
-            named = [slots[b, g, s] for s in range(depth)]
-
-            def pickup(c, held):
-                block = kv_all[c]
-                return tuple(lax.select(pick == c, block, old) for pick, old in zip(named, held))
-
-            nothing = jnp.zeros((BLK, 2 * LANES), BF)
-            found = lax.fori_loop(0, me * blocks, pickup, (nothing,) * depth)
             for s in range(depth):
-                near[(s + 1) * BLK : (s + 2) * BLK, :] = found[s]
-                shut = jnp.where(named[s] < 0, masked_low, 0.0)
-                bias = jnp.where(key_lane // BLK == s + 1, shut, bias)
-            score = lax.dot_general(qrows, near[:, :LANES], dims, preferred_element_type=F32) + bias
+                bias = jnp.where(key_lane // BLK == s + 1, shuts[b, g, s], bias)
+            score = lax.dot_general(qrows, near[g, :, :LANES], dims, preferred_element_type=F32) + bias
             score = jnp.where(hidden, masked_low, score)
             top = jnp.max(score, axis=1, keepdims=True)
             weight = jnp.exp(score - top)
-            prob = (weight / jnp.sum(weight, axis=1, keepdims=True)).astype(BF)
-            chosen_out = jnp.dot(prob, near[:, LANES:], preferred_element_type=F32)
+            prob = (weight * (1.0 / jnp.sum(weight, axis=1, keepdims=True))).astype(BF)
+            chosen_out = jnp.dot(prob, near[g, :, LANES:], preferred_element_type=F32)
 
             cols = [[], []]
             for i in range(per_group):
@@ -388,6 +428,7 @@
                 tile = g * (per_group // 2) + j
                 att[spot, tile * LANES : (tile + 1) * LANES] = jnp.where(lane64, even, odd).astype(BF)
 
+    oring.relay(early)
     oring.finish()
 
     def back(o):
@@ -452,9 +493,9 @@
                 pltpu.VMEM((count, width), BF),
                 pltpu.VMEM((n, wq.shape[0], cols), BF),
                 pltpu.VMEM((n,) + wo.shape, BF),
-                pltpu.VMEM(wg.shape, BF),
-                pltpu.VMEM(wck.shape, BF),
-                pltpu.VMEM(wcv.shape, BF),
+                pltpu.VMEM(wg.shape[::-1], BF),
+                pltpu.VMEM(wck.shape[::-1], BF),
+                pltpu.VMEM(wcv.shape[::-1], BF),
                 pltpu.VMEM((count, wq.shape[1]), F32),
                 pltpu.VMEM((2, count, LANES), F32),
                 pltpu.VMEM((n * blocks, BLK, 2 * LANES), BF),
@@ -462,10 +503,11 @@
                 pltpu.VMEM((n, PAD, 2 * LANES), BF),
                 pltpu.VMEM((count, wg.shape[1]), F32),
                 pltpu.VMEM((count, wq.shape[1]), BF),
-                pltpu.VMEM(((1 + depth) * BLK, 2 * LANES), BF),
+                pltpu.VMEM((groups, (1 + depth) * BLK, 2 * LANES), BF),
                 pltpu.VMEM((n, half, wo.shape[1]), BF),
                 pltpu.VMEM((n, half, wo.shape[1]), BF),
                 pltpu.SMEM((blocks, groups, depth), jnp.int32),
+                pltpu.SMEM((blocks, groups, depth), F32),
                 sem((8,)),
             ]
             + [sem(steps)] * 8
@@ -473,7 +515,7 @@
             compiler_params=pltpu.CompilerParams(
                 collective_id=0, has_side_effects=True, vmem_limit_bytes=60 * 1024 * 1024
             ),
-        )(seq_lengths, block_picks, tokens, wq, wk, wv, wg, wck, wcv, wo)
+        )(seq_lengths, block_picks, tokens, wq, wk, wv, wg.T, wck.T, wcv.T, wo)
 
     return jax.shard_map(
         body,

time: 93.8 us -> 83.7 us (0.89); the launches traced: 93.5 us -> 82.3 us
  local copies, waits for them, and re-layouts: 7.75 us -> 2.09 us
  Pallas kernels: 85 us -> 79.5 us
    unnamed x6 -> x1, local copies, waits for them, and re-layouts: 7.75 us -> 2.09 us
    pallas_call x1, Pallas kernels: 85 us -> 79.5 us  [body(): pl.pallas_call(functools.partial(kernel, sizes, share), out_shape=jax.Sha...]
where the time goes in v2:
time: 83.7 us; the launch traced here: 82.3 us
  Pallas kernels  79.5 us (95%)
  local copies, waits for them, and re-layouts  2.09 us (2%)
    pallas_call x1, Pallas kernels, body(): pl.pallas_call(functools.partial(kernel, sizes, share), out_shape=jax.Sha...  79.5 us
    unnamed x1, local copies, waits for them, and re-layouts  2.09 us

profile of v2, /device:TPU:23, one launch (start us, length us, event | category | flops | bytes accessed | tf_op | source)
XLA Modules:
  0.0 82.3 jit_solution(14360801099223291843)
XLA Ops:
  0.7 79.5 %shard_map.100 = bf16[1,192,2048]{2,1,0:T(8,128)(2,1)} custom-call(s32[1]{0:T(128)S(6)} %copy.12.seq_ref, s32[1,6,2,16]{3,2,1,0:T(2,128)} %picks_ref.1, bf16[1,384,2048]{2,1,0:T(8,128)(2,1)} %tokens_ref.1, bf16[512,512]{1,0:T(8,128)(2,1)} %wq_ref.1, bf16[512,128]{1,0:T(8,128)(2,1)} %wk_ref.1, bf16[512,128]{1,0:T(8,128)(2,1)} %wv_ref.1, ...), custom_call_target="tpu_custom_call" | custom-call | tf_op jit(solution)/shard_map/pallas_call | solution.py:486
  80.2 2.1 %copy.13 = bf16[1,192,2048]{2,1,0:T(8,128)(2,1)} copy(bf16[1,192,2048]{2,1,0:T(8,128)(2,1)} %shard_map.100) | data formatting | bytes 1572864
